TPU v7x, 32 devices: a whole 2x2x4 slice. The times are simulated.
32 devices in a mesh: tp: 16 (over z, y, core), dp: 2 (over x).
Axes of the slice: x: 2, y: 2, z: 4, core: 2. Of those that a mesh axis runs over, the one named last changes fastest.
Arguments:
- resid: bfloat16 [64, 2048], P('dp', 'tp'), may hold values from -6 to 6
- norm_gain: float32 [2, 2048], replicated, may hold values from 0.1 to 1.9
- w_query: bfloat16 [2, 2048, 2048], P(None, 'dp', 'tp'), may hold values from -0.125 to 0.125
- w_forget: bfloat16 [2, 2048, 2048], P(None, 'dp', 'tp'), may hold values from -0.125 to 0.125
- w_value: bfloat16 [2, 2048, 16, 128], P(None, 'dp', None, 'tp'), may hold values from -0.125 to 0.125
- w_gate: bfloat16 [2, 2048, 16, 128], P(None, 'dp', None, 'tp'), may hold values from -0.125 to 0.125
- gate_floor: float32 [2, 2048], replicated, may hold values from 0 to 0.9
- states: float32 [2, 64, 16, 128, 128], P(None, 'dp', None, 'tp'), may hold values from -1 to 1
- out_gain: float32 [2, 16, 128], P(None, None, 'tp'), may hold values from 0.1 to 1.9
- w_out: bfloat16 [2, 16, 128, 2048], P(None, None, 'tp'), may hold values from -0.125 to 0.125
Outputs:
- new_resid: bfloat16 [64, 2048], P('dp', 'tp')
- new_states: float32 [2, 64, 16, 128, 128], P(None, 'dp', None, 'tp')
All inputs are finite; a program needn't handle non-finite values.
Results may differ from a plain program's by a relative error of at most 0.029.
Values may be sent and summed in bfloat16 or wider, within the bound.
No kernel may reach another device: no remote copies, remote signals or barrier semaphores. Data moves between devices by JAX's collectives and lax.ppermute only.
A program may use at most 64 MiB of HBM per device.

v0:
```python
import jax
import jax.numpy as jnp
from jax import lax
from jax.sharding import PartitionSpec as P

BLOCKS = 2
epsilon = 1e-06


def shards(
    resid, norm_gain, w_query, w_forget, w_value, w_gate, gate_floor, states, out_gain, w_out
):
    residual = resid
    seq_local = resid.shape[0]
    heads = states.shape[2]
    slice_cols = states.shape[3]
    head_dim = states.shape[4]
    row_count = w_query.shape[1]
    new_list = []
    for layer in range(BLOCKS):
        gathered = lax.all_gather(residual, "tp", axis=1, tiled=True)
        resid_f32 = gathered.astype(jnp.float32)
        inv_rms = lax.rsqrt(jnp.mean(resid_f32 * resid_f32, axis=1, keepdims=True) + epsilon)
        scaled = (resid_f32 * norm_gain[layer]).astype(jnp.bfloat16)
        query_rows = w_query[layer]
        forget_rows = w_forget[layer]
        value_rows = w_value[layer].reshape(row_count, -1)
        gate_rows = w_gate[layer].reshape(row_count, -1)
        zero_sums = (
            jnp.zeros((seq_local, query_rows.shape[1]), jnp.float32),
            jnp.zeros((seq_local, forget_rows.shape[1]), jnp.float32),
            jnp.zeros((seq_local, value_rows.shape[1]), jnp.float32),
            jnp.zeros((seq_local, gate_rows.shape[1]), jnp.float32),
        )
        totals = zero_sums
        pieces = (
            lax.all_gather(query_rows, "dp", axis=0, tiled=True),
            lax.all_gather(forget_rows, "dp", axis=0, tiled=True),
            lax.all_gather(value_rows, "dp", axis=0, tiled=True),
            lax.all_gather(gate_rows, "dp", axis=0, tiled=True),
        )
        segments = pieces[0].shape[0] // row_count
        for part_index in range(segments):
            columns = lax.dynamic_slice_in_dim(scaled, part_index * row_count, row_count, 1)
            lo_row = part_index * row_count
            totals = tuple(
                (
                    total
                    + lax.optimization_barrier(
                        jnp.dot(
                            columns,
                            segment[lo_row : lo_row + row_count],
                            preferred_element_type=jnp.float32,
                        ).astype(jnp.bfloat16)
                    ).astype(jnp.float32)
                    for total, segment in zip(totals, pieces)
                )
            )
        queries, forget_pre, values, gate_pre = [
            (summed * inv_rms).astype(jnp.bfloat16) for summed in totals
        ]
        query_all, forget_all = (
            lax.all_gather(queries, "tp", axis=1, tiled=True),
            lax.all_gather(forget_pre, "tp", axis=1, tiled=True),
        )
        floor_now = gate_floor[layer]
        keep = floor_now + (1.0 - floor_now) * jax.nn.sigmoid(forget_all.astype(jnp.float32))
        keep = keep.reshape(seq_local, heads, head_dim)
        value_f32 = values.astype(jnp.float32).reshape(seq_local, heads, slice_cols)
        state_new = (
            keep[:, :, None, :] * states[layer]
            + (1.0 - keep)[:, :, None, :] * value_f32[:, :, :, None]
        )
        query_f32 = query_all.astype(jnp.float32).reshape(seq_local, heads, head_dim)
        readout = jnp.sum(query_f32[:, :, None, :] * state_new, axis=3)
        power_sum = lax.psum(jnp.sum(readout * readout, axis=2), "tp")
        mean_square = power_sum[..., None] / head_dim
        gate_f32 = gate_pre.astype(jnp.float32).reshape(seq_local, heads, slice_cols)
        normed = (
            readout * lax.rsqrt(mean_square + epsilon) * out_gain[layer] * jax.nn.silu(gate_f32)
        ).astype(jnp.bfloat16)
        flattened = normed.reshape(seq_local, heads * slice_cols)
        weight_out = w_out[layer].reshape(heads * slice_cols, -1)
        branch = lax.psum_scatter(
            lax.dot_general(
                weight_out, flattened, (((0,), (1,)), ((), ())), preferred_element_type=jnp.float32
            ),
            "tp",
            scatter_dimension=0,
            tiled=True,
        )
        residual = (residual.astype(jnp.float32) + branch.T).astype(jnp.bfloat16)
        new_list.append(state_new)
    return (residual, jnp.stack(new_list))


def solution(mesh):
    return jax.shard_map(
        shards,
        mesh=mesh,
        in_specs=(
            P("dp", "tp"),
            P(),
            P(None, "dp", "tp"),
            P(None, "dp", "tp"),
            P(None, "dp", None, "tp"),
            P(None, "dp", None, "tp"),
            P(),
            P(None, "dp", None, "tp", None),
            P(None, None, "tp"),
            P(None, None, "tp", None),
        ),
        out_specs=(P("dp", "tp"), P(None, "dp", None, "tp", None)),
        check_vma=False,
    )
```

profile of v0, /device:TPU:0, one launch (start us, length us, event | category | flops | bytes accessed | tf_op | source)
XLA Modules:
  0.0 405.7 jit_solution(406525206643660046)
XLA Ops:
  7.2 0.8 fusion.65
  8.0 23.7 %all_gather.42 = bf16[32,2048]{1,0:T(8,128)(2,1)S(1)} all-gather(bf16[32,128]{1,0:T(8,128)(2,1)} %param.10), channel_id=1, replica_groups=mesh['tp'=16,'dp'=2] {'tp'}, dimensions={1}, use_global_device_ids=true | all-gather | bytes 139264 | tf_op jit(solution)/shard_map/all_gather | solution.py:21
  31.8 1.1 fusion.62
  32.8 9.4 %all-gather = bf16[1,2048,128]{2,1,0:T(8,128)(2,1)S(1)} all-gather(bf16[1,1024,128]{2,1,0:T(8,128)(2,1)S(1)} %get-tuple-element.7), channel_id=2, replica_groups=mesh['tp'=16,'dp'=2] {'dp'}, dimensions={1}, use_global_device_ids=true | all-gather | bytes 786432 | tf_op jit(solution)/shard_map/all_gather | solution.py:37
  42.2 0.1 fusion.11
  42.3 0.2 convolution_convert_fusion.15
  42.5 0.2 convolution_convert_fusion.14
  42.7 8.5 %all-gather.1 = bf16[1,2048,128]{2,1,0:T(8,128)(2,1)S(1)} all-gather(bf16[1,1024,128]{2,1,0:T(8,128)(2,1)S(1)} %get-tuple-element.9), channel_id=3, replica_groups=mesh['tp'=16,'dp'=2] {'dp'}, dimensions={1}, use_global_device_ids=true | all-gather | bytes 786432 | tf_op jit(solution)/shard_map/all_gather | solution.py:38
  51.2 0.2 convolution_convert_fusion.13
  51.4 0.2 convolution_convert_fusion.12
  51.7 7.5 %all_gather.47 = bf16[2048,128]{0,1:T(8,128)(2,1)S(1)} all-gather(bf16[1024,128]{0,1:T(8,128)(2,1)S(1)} %get-tuple-element.10), channel_id=1, replica_groups=mesh['tp'=16,'dp'=2] {'dp'}, dimensions={0}, use_global_device_ids=true | all-gather | bytes 786432 | tf_op jit(solution)/shard_map/all_gather | solution.py:39
  59.2 0.2 convolution_convert_fusion.10
  59.3 0.2 convolution_convert_fusion.11
  59.6 7.0 %all_gather.48 = bf16[2048,128]{0,1:T(8,128)(2,1)S(1)} all-gather(bf16[1024,128]{0,1:T(8,128)(2,1)S(1)} %get-tuple-element.5), channel_id=1, replica_groups=mesh['tp'=16,'dp'=2] {'dp'}, dimensions={0}, use_global_device_ids=true | all-gather | bytes 786432 | tf_op jit(solution)/shard_map/all_gather | solution.py:40
  66.6 0.2 convolution_convert_fusion.8
  66.8 0.2 convolution_convert_fusion.9
  67.1 0.1 copy.27
  67.1 0.1 mul.312
  67.3 0.1 multiply_convert_fusion.7
  67.4 0.1 copy.24
  67.5 17.5 %all_gather.44 = bf16[32,2048]{1,0:T(8,128)(2,1)S(1)} all-gather(bf16[32,128]{1,0:T(8,128)(2,1)S(1)} %get-tuple-element.27), channel_id=1, replica_groups=mesh['tp'=16,'dp'=2] {'tp'}, dimensions={1}, use_global_device_ids=true | all-gather | bytes 139264 | tf_op jit(solution)/shard_map/all_gather | solution.py:63
  85.0 19.4 %all_gather.46 = bf16[32,2048]{1,0:T(8,128)(2,1)S(1)} all-gather(bf16[32,128]{1,0:T(8,128)(2,1)S(1)} %get-tuple-element.28), channel_id=1, replica_groups=mesh['tp'=16,'dp'=2] {'tp'}, dimensions={1}, use_global_device_ids=true | all-gather | bytes 139264 | tf_op jit(solution)/shard_map/all_gather | solution.py:64
  104.4 0.1 add_bitcast_fusion.1
  104.6 0.2 copy.25
  104.8 2.6 fusion.5
  107.4 0.1 multiply_reduce_fusion.1
  107.6 57.8 %psum.14 = f32[32,16]{1,0:T(8,128)S(1)} all-reduce(f32[32,16]{1,0:T(8,128)S(1)} %multiply_reduce_fusion.1), channel_id=1, replica_groups=mesh['tp'=16,'dp'=2] {'tp'}, use_global_device_ids=true, to_apply=%region_3.0 | all-reduce | flops 512 | bytes 4096 | tf_op jit(solution)/shard_map/psum | solution.py:76
  165.4 0.1 broadcast_multiply_fusion.1
  165.6 0.2 copy.26
  165.8 1.0 convolution_bitcast_fusion.1
  166.9 0.1 copy.32
  166.9 0.1 mul.345
  167.0 9.5 %all-gather.2 = bf16[1,2048,128]{2,1,0:T(8,128)(2,1)} all-gather(bf16[1,1024,128]{2,1,0:T(8,128)(2,1)S(1)} %get-tuple-element.6), channel_id=4, replica_groups=mesh['tp'=16,'dp'=2] {'dp'}, dimensions={1}, use_global_device_ids=true | all-gather | bytes 786432 | tf_op jit(solution)/shard_map/all_gather | solution.py:37
  176.5 9.2 %all-gather.3 = bf16[1,2048,128]{2,1,0:T(8,128)(2,1)S(1)} all-gather(bf16[1,1024,128]{2,1,0:T(8,128)(2,1)S(1)} %get-tuple-element.8), channel_id=5, replica_groups=mesh['tp'=16,'dp'=2] {'dp'}, dimensions={1}, use_global_device_ids=true | all-gather | bytes 786432 | tf_op jit(solution)/shard_map/all_gather | solution.py:38
  185.7 8.4 %all_gather.54 = bf16[2048,128]{0,1:T(8,128)(2,1)} all-gather(bf16[1024,128]{0,1:T(8,128)(2,1)S(1)} %get-tuple-element.11), channel_id=1, replica_groups=mesh['tp'=16,'dp'=2] {'dp'}, dimensions={0}, use_global_device_ids=true | all-gather | bytes 786432 | tf_op jit(solution)/shard_map/all_gather | solution.py:39
  194.1 7.1 %all_gather.55 = bf16[2048,128]{0,1:T(8,128)(2,1)} all-gather(bf16[1024,128]{0,1:T(8,128)(2,1)S(1)} %get-tuple-element.4), channel_id=1, replica_groups=mesh['tp'=16,'dp'=2] {'dp'}, dimensions={0}, use_global_device_ids=true | all-gather | bytes 786432 | tf_op jit(solution)/shard_map/all_gather | solution.py:40
  201.3 18.7 %reduce-scatter.3.cloned.1.call-done = f32[128,32]{0,1:T(8,128)} async-done(((f32[2048,32]{0,1:T(8,128)}), f32[128,32]{0,1:T(8,128)}) %reduce-scatter.3.cloned.1.call-update) | async-done | bytes 16400 | tf_op jit(solution)/shard_map/reduce_scatter | solution.py:84
  220.0 0.7 fusion.47
  220.7 19.7 %all_gather.49 = bf16[32,2048]{1,0:T(8,128)(2,1)S(1)} all-gather(bf16[32,128]{1,0:T(8,128)(2,1)S(1)} %fusion.47), channel_id=1, replica_groups=mesh['tp'=16,'dp'=2] {'tp'}, dimensions={1}, use_global_device_ids=true | all-gather | bytes 139264 | tf_op jit(solution)/shard_map/all_gather | solution.py:21
  240.4 0.2 fusion.13
  240.6 0.2 convolution_convert_fusion.5
  240.8 0.2 convolution_convert_fusion.4
  240.9 1.1 convolution_convert_fusion.3
  242.1 1.2 convolution_convert_fusion.2
  243.2 1.2 convolution_convert_fusion.1
  244.4 0.2 convolution_convert_fusion
  244.6 0.2 convolution_convert_fusion.6
  244.8 0.2 convolution_convert_fusion.7
  245.0 0.1 multiply_convert_fusion.3
  245.1 0.1 copy.29
  245.2 17.8 %all_gather.51 = bf16[32,2048]{1,0:T(8,128)(2,1)S(1)} all-gather(bf16[32,128]{1,0:T(8,128)(2,1)S(1)} %get-tuple-element.24), channel_id=1, replica_groups=mesh['tp'=16,'dp'=2] {'tp'}, dimensions={1}, use_global_device_ids=true | all-gather | bytes 139264 | tf_op jit(solution)/shard_map/all_gather | solution.py:63
  263.0 19.1 %all_gather.53 = bf16[32,2048]{1,0:T(8,128)(2,1)S(1)} all-gather(bf16[32,128]{1,0:T(8,128)(2,1)S(1)} %get-tuple-element.25), channel_id=1, replica_groups=mesh['tp'=16,'dp'=2] {'tp'}, dimensions={1}, use_global_device_ids=true | all-gather | bytes 139264 | tf_op jit(solution)/shard_map/all_gather | solution.py:64
  282.1 0.1 add_bitcast_fusion
  282.3 0.2 copy.30
  282.5 2.6 fusion.2
  285.1 0.1 multiply_reduce_fusion
  285.2 57.8 %psum.15 = f32[32,16]{1,0:T(8,128)S(1)} all-reduce(f32[32,16]{1,0:T(8,128)S(1)} %multiply_reduce_fusion), channel_id=1, replica_groups=mesh['tp'=16,'dp'=2] {'tp'}, use_global_device_ids=true, to_apply=%region_8.9 | all-reduce | flops 512 | bytes 4096 | tf_op jit(solution)/shard_map/psum | solution.py:76
  343.0 0.1 broadcast_multiply_fusion
  343.2 0.2 copy.31
  343.4 1.0 convolution_bitcast_fusion
  344.4 3.5 multiply_add_fusion.1
  348.0 2.3 pad_maximum_fusion
  350.2 47.3 %reduce-scatter.5.cloned.1.call-done = f32[128,32]{0,1:T(8,128)} async-done(((f32[2048,32]{0,1:T(8,128)}), f32[128,32]{0,1:T(8,128)}) %reduce-scatter.5.cloned.1.call-update) | async-done | bytes 16400 | tf_op jit(solution)/shard_map/reduce_scatter | solution.py:84
  397.5 1.3 fusion.46
  (41 shorter events, 0.8 us)
Async XLA Ops:
  7.2 35.5 %copy-start.3 = (bf16[2,1024,128]{2,1,0:T(8,128)(2,1)S(1)}, bf16[2,1024,128]{2,1,0:T(8,128)(2,1)}, u32[]{:S(2)}) copy-start(bf16[2,1024,128]{2,1,0:T(8,128)(2,1)} %param.13) | copy-start | bytes 1572868
  7.2 212.8 %reduce-scatter.3.cloned.1.call-start = ((), (), s32[]{:S(2)}) async-start(), calls=%async_computation.2 | async-start | bytes 278528 | tf_op jit(solution)/shard_map/reduce_scatter | solution.py:84
  32.8 18.8 %copy-start.4 = (bf16[2,1024,16,8]{1,3,2,0:T(8,128)(2,1)S(1)}, bf16[2,1024,16,8]{1,3,2,0:T(8,128)(2,1)}, u32[]{:S(2)}) copy-start(bf16[2,1024,16,8]{1,3,2,0:T(8,128)(2,1)} %param.14) | copy-start | bytes 1572868
  42.7 16.8 %copy-start.5 = (bf16[2,1024,16,8]{1,3,2,0:T(8,128)(2,1)S(1)}, bf16[2,1024,16,8]{1,3,2,0:T(8,128)(2,1)}, u32[]{:S(2)}) copy-start(bf16[2,1024,16,8]{1,3,2,0:T(8,128)(2,1)} %param.15) | copy-start | bytes 1572868
  51.6 15.4 %copy-start.8 = (f32[2,16,8]{1,2,0:T(8,128)S(1)}, f32[2,16,8]{1,2,0:T(8,128)}, u32[]{:S(2)}) copy-start(f32[2,16,8]{1,2,0:T(8,128)} %param.18) | copy-start | bytes 3076
  51.6 15.6 %copy-start.7 = (f32[2,2048]{1,0:T(2,128)S(1)}, f32[2,2048]{1,0:T(2,128)}, u32[]{:S(2)}) copy-start(f32[2,2048]{1,0:T(2,128)} %param.16) | copy-start | bytes 49156
  104.8 61.0 %copy-start = (bf16[2,16,8,2048]{3,2,1,0:T(8,128)(2,1)S(1)}, bf16[2,16,8,2048]{3,2,1,0:T(8,128)(2,1)}, u32[]{:S(2)}) copy-start(bf16[2,16,8,2048]{3,2,1,0:T(8,128)(2,1)} %param.19) | copy-start | bytes 3145732
  165.8 54.2 %copy-start.6 = (bf16[32,128]{1,0:T(8,128)(2,1)S(1)}, bf16[32,128]{1,0:T(8,128)(2,1)}, u32[]{:S(2)}) copy-start(bf16[32,128]{1,0:T(8,128)(2,1)} %param.10) | copy-start | bytes 24580
  166.8 230.7 %reduce-scatter.5.cloned.1.call-start = ((), (), s32[]{:S(2)}) async-start(), calls=%async_computation.3 | async-start | bytes 278528 | tf_op jit(solution)/shard_map/reduce_scatter | solution.py:84
  185.7 58.9 %copy-start.1 = (bf16[1,2048,128]{2,1,0:T(8,128)(2,1)S(1)}, bf16[1,2048,128]{2,1,0:T(8,128)(2,1)}, u32[]{:S(2)}) copy-start(bf16[1,2048,128]{2,1,0:T(8,128)(2,1)} %all-gather.2) | copy-start | bytes 1572868
  201.3 43.1 %copy-start.2 = (bf16[2048,128]{0,1:T(8,128)(2,1)S(1)}, bf16[2048,128]{0,1:T(8,128)(2,1)}, u32[]{:S(2)}) copy-start(bf16[2048,128]{0,1:T(8,128)(2,1)} %all_gather.55) | copy-start | bytes 1572868
Sparse Core Ops, SparseCore 0:
  166.9 52.9 reduce-scatter.2
  344.5 52.9 reduce-scatter.4
where the time goes:
time: 406 us
  blocking collectives  300 us (74%)
  waiting for transfers between devices  66 us (16%)
  other arithmetic  14.4 us (4%)
  between operations  14.4 us (4%)
  matrix products  7.68 us (2%)
    psum x2, blocking collectives, shards(): power_sum = lax.psum(jnp.sum(readout * readout, axis=2), 'tp')  116 us
    reduce_scatter x2, waiting for transfers between devices, shards(): lax.psum_scatter(lax.dot_general(weight_out, flattened, (((0,), (1,)), ((...  66 us
    all_gather x2, blocking collectives, shards(): gathered = lax.all_gather(residual, 'tp', axis=1, tiled=True)  43.5 us
    all_gather x2, blocking collectives, shards(): lax.all_gather(forget_pre, 'tp', axis=1, tiled=True)  38.5 us
    all_gather x2, blocking collectives, shards(): lax.all_gather(queries, 'tp', axis=1, tiled=True)  35.3 us
    all_gather x2, blocking collectives, shards(): lax.all_gather(query_rows, 'dp', axis=0, tiled=True)  18.8 us
    all_gather x2, blocking collectives, shards(): lax.all_gather(forget_rows, 'dp', axis=0, tiled=True)  17.7 us
    all_gather x2, blocking collectives, shards(): lax.all_gather(value_rows, 'dp', axis=0, tiled=True)  15.9 us
  transfers between devices with their start and end apart: 2, of which 2 were waited for; matrix products, arithmetic and copies ran while one was open for 1% of the time, Pallas kernels for 0%

commit v1 on v0

--- a/solution.py
+++ b/solution.py
@@ -73,7 +73,9 @@
         )
         query_f32 = query_all.astype(jnp.float32).reshape(seq_local, heads, head_dim)
         readout = jnp.sum(query_f32[:, :, None, :] * state_new, axis=3)
-        power_sum = lax.psum(jnp.sum(readout * readout, axis=2), "tp")
+        content = jnp.sum(readout * readout, axis=2)
+        block_now = lax.all_gather(content, "tp")
+        power_sum = jnp.sum(block_now, axis=0)
         mean_square = power_sum[..., None] / head_dim
         gate_f32 = gate_pre.astype(jnp.float32).reshape(seq_local, heads, slice_cols)
         normed = (

time: 406 us -> 329 us (0.81)
  blocking collectives: 300 us -> 218 us
    psum x2 -> x0, blocking collectives: 116 us -> none  [shards(): power_sum = lax.psum(jnp.sum(readout * readout, axis=2), 'tp')]
    all_gather x0 -> x2, blocking collectives: none -> 35.6 us  [shards(): block_now = lax.all_gather(content, 'tp')]
  transfers between devices with their start and end apart: 2 -> 2, of which waited for: 2 -> 2; matrix products, arithmetic and copies ran while one was open for 1% -> 2% of each run, Pallas kernels for 0% -> 0%
where the time goes in v1:
time: 329 us; the launch traced here: 328 us
  blocking collectives  218 us (66%)
  waiting for transfers between devices  69.9 us (21%)
  between operations  14.4 us (4%)
  other arithmetic  14.2 us (4%)
  matrix products  7.67 us (2%)
  local copies, waits for them, and re-layouts  4.01 us (1%)
    reduce_scatter x2, waiting for transfers between devices, shards(): lax.psum_scatter(lax.dot_general(weight_out, flattened, (((0,), (1,)), ((...  69.9 us
    all_gather x2, blocking collectives, shards(): gathered = lax.all_gather(residual, 'tp', axis=1, tiled=True)  43.5 us
    all_gather x2, blocking collectives, shards(): lax.all_gather(forget_pre, 'tp', axis=1, tiled=True)  38.5 us
    all_gather x2, blocking collectives, shards(): block_now = lax.all_gather(content, 'tp')  35.6 us
    all_gather x2, blocking collectives, shards(): lax.all_gather(queries, 'tp', axis=1, tiled=True)  35.3 us
    all_gather x2, blocking collectives, shards(): lax.all_gather(query_rows, 'dp', axis=0, tiled=True)  18.7 us
    all_gather x2, blocking collectives, shards(): lax.all_gather(forget_rows, 'dp', axis=0, tiled=True)  16.8 us
    all_gather x2, blocking collectives, shards(): lax.all_gather(value_rows, 'dp', axis=0, tiled=True)  15.2 us
  transfers between devices with their start and end apart: 2, of which 2 were waited for; matrix products, arithmetic and copies ran while one was open for 2% of the time, Pallas kernels for 0%

profile of v1, /device:TPU:0, one launch (start us, length us, event | category | flops | bytes accessed | tf_op | source)
XLA Modules:
  0.0 328.1 jit_solution(10134821384057871304)
XLA Ops:
  7.2 0.8 fusion.65
  8.0 23.7 %all_gather.54 = bf16[32,2048]{1,0:T(8,128)(2,1)S(1)} all-gather(bf16[32,128]{1,0:T(8,128)(2,1)} %param.10), channel_id=1, replica_groups=mesh['tp'=16,'dp'=2] {'tp'}, dimensions={1}, use_global_device_ids=true | all-gather | bytes 139264 | tf_op jit(solution)/shard_map/all_gather | solution.py:21
  31.8 1.1 fusion.62
  32.8 9.4 %all-gather = bf16[1,2048,128]{2,1,0:T(8,128)(2,1)S(1)} all-gather(bf16[1,1024,128]{2,1,0:T(8,128)(2,1)S(1)} %get-tuple-element.7), channel_id=2, replica_groups=mesh['tp'=16,'dp'=2] {'dp'}, dimensions={1}, use_global_device_ids=true | all-gather | bytes 786432 | tf_op jit(solution)/shard_map/all_gather | solution.py:37
  42.2 0.2 fusion.11
  42.3 0.2 convolution_convert_fusion.15
  42.5 0.2 convolution_convert_fusion.14
  42.7 8.5 %all-gather.1 = bf16[1,2048,128]{2,1,0:T(8,128)(2,1)S(1)} all-gather(bf16[1,1024,128]{2,1,0:T(8,128)(2,1)S(1)} %get-tuple-element.9), channel_id=3, replica_groups=mesh['tp'=16,'dp'=2] {'dp'}, dimensions={1}, use_global_device_ids=true | all-gather | bytes 786432 | tf_op jit(solution)/shard_map/all_gather | solution.py:38
  51.2 0.2 convolution_convert_fusion.13
  51.4 0.2 convolution_convert_fusion.12
  51.7 7.5 %all_gather.59 = bf16[2048,128]{0,1:T(8,128)(2,1)S(1)} all-gather(bf16[1024,128]{0,1:T(8,128)(2,1)S(1)} %get-tuple-element.10), channel_id=1, replica_groups=mesh['tp'=16,'dp'=2] {'dp'}, dimensions={0}, use_global_device_ids=true | all-gather | bytes 786432 | tf_op jit(solution)/shard_map/all_gather | solution.py:39
  59.2 0.2 convolution_convert_fusion.10
  59.3 0.2 convolution_convert_fusion.11
  59.6 7.0 %all_gather.62 = bf16[2048,128]{0,1:T(8,128)(2,1)S(1)} all-gather(bf16[1024,128]{0,1:T(8,128)(2,1)S(1)} %get-tuple-element.5), channel_id=1, replica_groups=mesh['tp'=16,'dp'=2] {'dp'}, dimensions={0}, use_global_device_ids=true | all-gather | bytes 786432 | tf_op jit(solution)/shard_map/all_gather | solution.py:40
  66.6 0.2 convolution_convert_fusion.8
  66.8 0.2 convolution_convert_fusion.9
  67.1 0.1 mul.312
  67.3 0.1 multiply_convert_fusion.7
  67.4 0.1 copy.54
  67.5 17.5 %all_gather.56 = bf16[32,2048]{1,0:T(8,128)(2,1)S(1)} all-gather(bf16[32,128]{1,0:T(8,128)(2,1)S(1)} %get-tuple-element.27), channel_id=1, replica_groups=mesh['tp'=16,'dp'=2] {'tp'}, dimensions={1}, use_global_device_ids=true | all-gather | bytes 139264 | tf_op jit(solution)/shard_map/all_gather | solution.py:63
  85.0 19.4 %all_gather.58 = bf16[32,2048]{1,0:T(8,128)(2,1)S(1)} all-gather(bf16[32,128]{1,0:T(8,128)(2,1)S(1)} %get-tuple-element.28), channel_id=1, replica_groups=mesh['tp'=16,'dp'=2] {'tp'}, dimensions={1}, use_global_device_ids=true | all-gather | bytes 139264 | tf_op jit(solution)/shard_map/all_gather | solution.py:64
  104.4 0.1 add_bitcast_fusion.1
  104.6 0.2 copy.55
  104.8 2.6 fusion.5
  107.4 0.2 copy.56
  107.6 17.8 %all-gather.6 = f32[16,32,16]{1,2,0:T(8,128)S(1)} all-gather(f32[1,32,16]{1,2,0:T(8,128)S(1)} %bitcast.102), channel_id=4, replica_groups=mesh['tp'=16,'dp'=2] {'tp'}, dimensions={0}, use_global_device_ids=true | all-gather | bytes 34816 | tf_op jit(solution)/shard_map/all_gather | solution.py:77
  125.5 0.1 copy.58
  125.5 0.1 broadcast_multiply_fusion.1
  125.7 0.2 copy.59
  125.9 1.0 convolution_bitcast_fusion.1
  127.0 0.1 mul.345
  127.1 9.3 %all-gather.3 = bf16[1,2048,128]{2,1,0:T(8,128)(2,1)} all-gather(bf16[1,1024,128]{2,1,0:T(8,128)(2,1)S(1)} %get-tuple-element.6), channel_id=5, replica_groups=mesh['tp'=16,'dp'=2] {'dp'}, dimensions={1}, use_global_device_ids=true | all-gather | bytes 786432 | tf_op jit(solution)/shard_map/all_gather | solution.py:37
  136.5 8.3 %all-gather.4 = bf16[1,2048,128]{2,1,0:T(8,128)(2,1)S(1)} all-gather(bf16[1,1024,128]{2,1,0:T(8,128)(2,1)S(1)} %get-tuple-element.8), channel_id=6, replica_groups=mesh['tp'=16,'dp'=2] {'dp'}, dimensions={1}, use_global_device_ids=true | all-gather | bytes 786432 | tf_op jit(solution)/shard_map/all_gather | solution.py:38
  144.8 7.7 %all_gather.68 = bf16[2048,128]{0,1:T(8,128)(2,1)} all-gather(bf16[1024,128]{0,1:T(8,128)(2,1)S(1)} %get-tuple-element.11), channel_id=1, replica_groups=mesh['tp'=16,'dp'=2] {'dp'}, dimensions={0}, use_global_device_ids=true | all-gather | bytes 786432 | tf_op jit(solution)/shard_map/all_gather | solution.py:39
  152.5 7.1 %all_gather.71 = bf16[2048,128]{0,1:T(8,128)(2,1)} all-gather(bf16[1024,128]{0,1:T(8,128)(2,1)S(1)} %get-tuple-element.4), channel_id=1, replica_groups=mesh['tp'=16,'dp'=2] {'dp'}, dimensions={0}, use_global_device_ids=true | all-gather | bytes 786432 | tf_op jit(solution)/shard_map/all_gather | solution.py:40
  159.7 21.5 %reduce-scatter.3.cloned.1.call-done = f32[128,32]{0,1:T(8,128)} async-done(((f32[2048,32]{0,1:T(8,128)}), f32[128,32]{0,1:T(8,128)}) %reduce-scatter.3.cloned.1.call-update) | async-done | bytes 16400 | tf_op jit(solution)/shard_map/reduce_scatter | solution.py:86
  181.2 0.7 fusion.47
  181.9 19.8 %all_gather.63 = bf16[32,2048]{1,0:T(8,128)(2,1)S(1)} all-gather(bf16[32,128]{1,0:T(8,128)(2,1)S(1)} %fusion.47), channel_id=1, replica_groups=mesh['tp'=16,'dp'=2] {'tp'}, dimensions={1}, use_global_device_ids=true | all-gather | bytes 139264 | tf_op jit(solution)/shard_map/all_gather | solution.py:21
  201.7 0.2 fusion.13
  201.8 0.2 convolution_convert_fusion.5
  202.0 0.2 convolution_convert_fusion.4
  202.1 1.1 convolution_convert_fusion.3
  203.3 1.2 convolution_convert_fusion.2
  204.4 1.2 convolution_convert_fusion.1
  205.6 0.2 convolution_convert_fusion
  205.8 0.2 convolution_convert_fusion.6
  206.0 0.2 convolution_convert_fusion.7
  206.2 0.1 multiply_convert_fusion.3
  206.3 0.1 copy.62
  206.4 17.8 %all_gather.65 = bf16[32,2048]{1,0:T(8,128)(2,1)S(1)} all-gather(bf16[32,128]{1,0:T(8,128)(2,1)S(1)} %get-tuple-element.24), channel_id=1, replica_groups=mesh['tp'=16,'dp'=2] {'tp'}, dimensions={1}, use_global_device_ids=true | all-gather | bytes 139264 | tf_op jit(solution)/shard_map/all_gather | solution.py:63
  224.2 19.1 %all_gather.67 = bf16[32,2048]{1,0:T(8,128)(2,1)S(1)} all-gather(bf16[32,128]{1,0:T(8,128)(2,1)S(1)} %get-tuple-element.25), channel_id=1, replica_groups=mesh['tp'=16,'dp'=2] {'tp'}, dimensions={1}, use_global_device_ids=true | all-gather | bytes 139264 | tf_op jit(solution)/shard_map/all_gather | solution.py:64
  243.4 0.1 add_bitcast_fusion
  243.5 0.2 copy.63
  243.7 2.6 fusion.2
  246.3 0.2 copy.64
  246.5 17.8 %all-gather.7 = f32[16,32,16]{1,2,0:T(8,128)S(1)} all-gather(f32[1,32,16]{1,2,0:T(8,128)S(1)} %bitcast.103), channel_id=7, replica_groups=mesh['tp'=16,'dp'=2] {'tp'}, dimensions={0}, use_global_device_ids=true | all-gather | bytes 34816 | tf_op jit(solution)/shard_map/all_gather | solution.py:77
  264.3 0.1 copy.66
  264.4 0.1 broadcast_multiply_fusion
  264.5 0.2 copy.67
  264.7 1.0 convolution_bitcast_fusion
  265.7 3.5 %multiply_add_fusion.1 = (f32[1,32,16,8,128]{4,3,2,1,0:T(8,128)S(1)}, f32[1,32,16,8,128]{4,3,2,1,0:T(8,128)S(1)}) fusion(f32[2,32,16,8,128]{4,3,2,1,0:T(8,128)} %param.17, f32[32,16,8]{2,1,0:T(8,128)S(1)} %copy.55, f32[32,16,128]{2,1,0:T(8,128)S(1)} %broadcast_subtract_fusion.1, f32[32,16,128]{2,1,0:T(8,128)S(1)} %bitcast.93, f32[32,16,8]{2,1,0:T(8,128)S(1)} %copy.63, ...), kind=kLoop, calls=%fused_computation.12 | loop fusion | flops 3145728 | bytes 9469952 | tf_op jit(solution)/shard_map/add | solution.py:71
  269.3 2.3 pad_maximum_fusion
  271.5 48.4 %reduce-scatter.5.cloned.1.call-done = f32[128,32]{0,1:T(8,128)} async-done(((f32[2048,32]{0,1:T(8,128)}), f32[128,32]{0,1:T(8,128)}) %reduce-scatter.5.cloned.1.call-update) | async-done | bytes 16400 | tf_op jit(solution)/shard_map/reduce_scatter | solution.py:86
  319.9 1.3 fusion.46
  (47 shorter events, 1.0 us)
Async XLA Ops:
  7.2 35.5 %copy-start.3 = (bf16[2,1024,128]{2,1,0:T(8,128)(2,1)S(1)}, bf16[2,1024,128]{2,1,0:T(8,128)(2,1)}, u32[]{:S(2)}) copy-start(bf16[2,1024,128]{2,1,0:T(8,128)(2,1)} %param.13) | copy-start | bytes 1572868
  7.2 174.0 %reduce-scatter.3.cloned.1.call-start = ((), (), s32[]{:S(2)}) async-start(), calls=%async_computation.2 | async-start | bytes 278528 | tf_op jit(solution)/shard_map/reduce_scatter | solution.py:86
  32.8 18.8 %copy-start.4 = (bf16[2,1024,16,8]{1,3,2,0:T(8,128)(2,1)S(1)}, bf16[2,1024,16,8]{1,3,2,0:T(8,128)(2,1)}, u32[]{:S(2)}) copy-start(bf16[2,1024,16,8]{1,3,2,0:T(8,128)(2,1)} %param.14) | copy-start | bytes 1572868
  42.7 16.8 %copy-start.5 = (bf16[2,1024,16,8]{1,3,2,0:T(8,128)(2,1)S(1)}, bf16[2,1024,16,8]{1,3,2,0:T(8,128)(2,1)}, u32[]{:S(2)}) copy-start(bf16[2,1024,16,8]{1,3,2,0:T(8,128)(2,1)} %param.15) | copy-start | bytes 1572868
  51.6 15.4 %copy-start.8 = (f32[2,16,8]{1,2,0:T(8,128)S(1)}, f32[2,16,8]{1,2,0:T(8,128)}, u32[]{:S(2)}) copy-start(f32[2,16,8]{1,2,0:T(8,128)} %param.18) | copy-start | bytes 3076
  51.6 15.6 %copy-start.7 = (f32[2,2048]{1,0:T(2,128)S(1)}, f32[2,2048]{1,0:T(2,128)}, u32[]{:S(2)}) copy-start(f32[2,2048]{1,0:T(2,128)} %param.16) | copy-start | bytes 49156
  104.8 21.1 %copy-start = (bf16[2,16,8,2048]{3,2,1,0:T(8,128)(2,1)S(1)}, bf16[2,16,8,2048]{3,2,1,0:T(8,128)(2,1)}, u32[]{:S(2)}) copy-start(bf16[2,16,8,2048]{3,2,1,0:T(8,128)(2,1)} %param.19) | copy-start | bytes 3145732
  125.9 55.3 %copy-start.6 = (bf16[32,128]{1,0:T(8,128)(2,1)S(1)}, bf16[32,128]{1,0:T(8,128)(2,1)}, u32[]{:S(2)}) copy-start(bf16[32,128]{1,0:T(8,128)(2,1)} %param.10) | copy-start | bytes 24580
  126.9 193.0 %reduce-scatter.5.cloned.1.call-start = ((), (), s32[]{:S(2)}) async-start(), calls=%async_computation.3 | async-start | bytes 278528 | tf_op jit(solution)/shard_map/reduce_scatter | solution.py:86
  144.8 61.0 %copy-start.1 = (bf16[1,2048,128]{2,1,0:T(8,128)(2,1)S(1)}, bf16[1,2048,128]{2,1,0:T(8,128)(2,1)}, u32[]{:S(2)}) copy-start(bf16[1,2048,128]{2,1,0:T(8,128)(2,1)} %all-gather.3) | copy-start | bytes 1572868
  159.7 46.0 %copy-start.2 = (bf16[2048,128]{0,1:T(8,128)(2,1)S(1)}, bf16[2048,128]{0,1:T(8,128)(2,1)}, u32[]{:S(2)}) copy-start(bf16[2048,128]{0,1:T(8,128)(2,1)} %all_gather.71) | copy-start | bytes 1572868
Sparse Core Ops, SparseCore 0:
  127.0 54.0 reduce-scatter.2
  265.8 54.0 reduce-scatter.4
